TPU v7x, 32 devices: a whole 2x2x4 slice. The times are simulated.
32 devices in a mesh: ep: 4 (over z), tp: 8 (over y, x, core).
Axes of the slice: x: 2, y: 2, z: 4, core: 2. Of those that a mesh axis runs over, the one named last changes fastest.
Arguments:
- hidden: bfloat16 [64, 4096], P('ep', 'tp'), may hold values from -6 to 6
- norm_gain: float32 [4096], replicated, may hold values from 0.1 to 1.9
- routes: int32 [64, 4], P('ep'), may hold values from 0 to 7, all different within a row; in each aligned block of 16 rows (0 to 15, 16 to 31, ...) at most 13 rows name the same one
- route_weights: float32 [64, 4], P('ep'), may hold values from 0.1 to 1
- gate_weight: bfloat16 [8, 1024, 4096], P('ep', 'tp'), may hold values from -0.09375 to 0.09375
- up_weight: bfloat16 [8, 1024, 4096], P('ep', 'tp'), may hold values from -0.09375 to 0.09375
- down_weight: bfloat16 [8, 1024, 4096], P('ep', 'tp'), may hold values from -0.25 to 0.25
- shared_gate: bfloat16 [1024, 4096], P('tp'), may hold values from -0.09375 to 0.09375
- shared_up: bfloat16 [1024, 4096], P('tp'), may hold values from -0.09375 to 0.09375
- shared_down: bfloat16 [1024, 4096], P('tp'), may hold values from -0.25 to 0.25
Outputs:
- mixed: bfloat16 [64, 4096], P('ep', 'tp')
Inputs may be any that keep to these rules, and one draw needn't show every extreme that they name: `routes`: each row names 4 different experts; among the rows of one index of ep (aligned blocks of 16 rows) no expert is named more than 13 times, a bound that some block reaches.
All inputs are finite; a program needn't handle non-finite values.
Results may differ from a plain program's by a relative error of at most 0.017.
Values may be sent and summed in bfloat16 or wider, within the bound.
A program may use at most 64 MiB of HBM per device.

v0:
```python
import jax
import jax.numpy as jnp
from jax import lax
from jax.sharding import PartitionSpec as P

norm_eps = 1e-06


def norm_rows(gathered, norm_gain):
    values = gathered.astype(jnp.float32)
    inv_scale = lax.rsqrt(jnp.mean(values * values, axis=-1, keepdims=True) + norm_eps)
    return (values * inv_scale * norm_gain).astype(jnp.bfloat16)


def slot_table(routes, expert_count, capacity):
    onehot = (
        routes[:, :, None] == jnp.arange(expert_count, dtype=jnp.int32)[None, None, :]
    ).astype(jnp.int32)
    used_mask = jnp.sum(onehot, axis=1)
    before = jnp.cumsum(used_mask, axis=0) - used_mask
    slot_rank = jnp.sum(onehot * before[:, None, :], axis=2)
    return routes * capacity + slot_rank


def per_device(
    hidden,
    norm_gain,
    routes,
    route_weights,
    gate_weight,
    up_weight,
    down_weight,
    shared_gate,
    shared_up,
    shared_down,
):
    width_group = lax.axis_size("tp")
    down_local = lax.all_to_all(down_weight, "tp", split_axis=2, concat_axis=1, tiled=True)
    gathered = lax.all_gather(hidden, "tp", axis=1, tiled=True)
    normed = norm_rows(gathered, norm_gain)
    tok_rows, top_count = routes.shape
    local_experts = gate_weight.shape[0]
    groups = lax.axis_size("ep")
    experts = local_experts * groups
    capacity = min(tok_rows, 3 * tok_rows * top_count // (2 * experts) + 1)
    full_width = gathered.shape[1]
    slot_ids = slot_table(routes, experts, capacity)
    slot_range = jnp.arange(experts * capacity, dtype=jnp.int32)
    matches = slot_ids[:, :, None] == slot_range[None, None, :]
    combine = jnp.sum(jnp.where(matches, route_weights[:, :, None], 0.0), axis=1)
    select = jnp.sum(
        (slot_range[:, None, None] == slot_ids[None, :, :]).astype(jnp.bfloat16), axis=2
    )
    packed = jnp.dot(select, normed, preferred_element_type=jnp.float32).astype(jnp.bfloat16)
    packed = packed.reshape(groups, local_experts, capacity, full_width)
    arrived = lax.all_to_all(packed, "ep", split_axis=0, concat_axis=0, tiled=True)
    gate_vals = jnp.einsum(
        "secd,efd->secf", arrived, gate_weight, preferred_element_type=jnp.float32
    )
    up_vals = jnp.einsum("secd,efd->secf", arrived, up_weight, preferred_element_type=jnp.float32)
    inner_vals = (jax.nn.silu(gate_vals) * up_vals).astype(jnp.bfloat16)
    dims = (((1,), (1,)), ((), ()))
    shared_gates = lax.dot_general(normed, shared_gate, dims, preferred_element_type=jnp.float32)
    shared_ups = lax.dot_general(normed, shared_up, dims, preferred_element_type=jnp.float32)
    shared_inner = (jax.nn.silu(shared_gates) * shared_ups).astype(jnp.bfloat16)
    shared_part = jnp.dot(shared_inner, shared_down, preferred_element_type=jnp.float32).astype(
        jnp.bfloat16
    )
    inner_whole = lax.all_gather(inner_vals, "tp", axis=3, tiled=True)
    slots, _, cap_rows, hidden_units = inner_whole.shape
    block_units = hidden_units // width_group
    inner_blocks = inner_whole.reshape(slots, local_experts, cap_rows, width_group, block_units)
    down_blocks = down_local.reshape(local_experts, width_group, block_units, down_local.shape[2])
    block_sums = jnp.einsum(
        "secpf,epfd->secpd", inner_blocks, down_blocks, preferred_element_type=jnp.float32
    ).astype(jnp.bfloat16)
    answers = jnp.sum(block_sums.astype(jnp.float32), axis=3).astype(jnp.bfloat16)
    shared_sum = lax.psum_scatter(shared_part, "tp", scatter_dimension=1, tiled=True).astype(
        jnp.float32
    )
    returned = lax.all_to_all(answers, "ep", split_axis=0, concat_axis=0, tiled=True)
    flat_rows = returned.reshape(-1, returned.shape[3]).astype(jnp.float32)
    routed = jnp.dot(combine, flat_rows, precision=lax.Precision.HIGHEST)
    return (routed + shared_sum).astype(jnp.bfloat16)


def solution(mesh):
    in_specs = (
        P("ep", "tp"),
        P(),
        P("ep", None),
        P("ep", None),
        P("ep", "tp", None),
        P("ep", "tp", None),
        P("ep", "tp", None),
        P("tp", None),
        P("tp", None),
        P("tp", None),
    )
    out_specs = P("ep", "tp")
    return jax.shard_map(
        per_device, mesh=mesh, in_specs=in_specs, out_specs=out_specs, check_vma=False
    )
```

profile of v0, /device:TPU:0, one launch (start us, length us, event | category | flops | bytes accessed | tf_op | source)
XLA Modules:
  0.0 113.9 jit_solution(8584589679115222297)
XLA Ops:
  6.5 0.8 convert_reduce_fusion
  7.4 0.1 copy.40
  7.5 0.1 copy.42
  7.6 0.7 select_reduce_fusion.1
  8.3 0.7 multiply_add_fusion
  9.0 0.1 fusion.33
  9.0 10.9 %all_gather.6 = bf16[16,4096]{1,0:T(8,128)(2,1)S(1)} all-gather(bf16[16,512]{1,0:T(8,128)(2,1)} %param.10), channel_id=1, replica_groups=mesh['ep'=4,'tp'=8] {'tp'}, dimensions={1}, use_global_device_ids=true | all-gather | bytes 147456 | tf_op jit(solution)/shard_map/all_gather | solution.py:39
  19.9 0.1 fusion.28
  20.1 2.1 %convolution_convert_fusion = bf16[104,4096]{1,0:T(8,128)(2,1)} fusion(bf16[104,16]{0,1:T(8,128)(2,1)S(1)} %fusion.33, bf16[16,4096]{1,0:T(8,128)(2,1)S(1)} %all_gather.6, f32[4096]{0:T(1024)} %param.11, f32[16]{0:T(128)S(1)} %add_rsqrt_fusion), kind=kOutput, calls=%fused_computation | convolution fusion | flops 14319616 | bytes 1002816 | tf_op jit(solution)/shard_map/dot_general | solution.py:54
  22.2 1.4 %reshape.33 = bf16[4,2,13,4096]{3,2,1,0:T(8,128)(2,1)S(1)} reshape(bf16[104,4096]{1,0:T(8,128)(2,1)} %convolution_convert_fusion) | data formatting | bytes 1703936 | tf_op jit(solution)/shard_map/reshape | solution.py:55
  23.6 1.8 %copy.43 = bf16[4,2,13,4096]{3,1,2,0:T(2,128)(2,1)} copy(bf16[4,2,13,4096]{3,2,1,0:T(8,128)(2,1)S(1)} %reshape.33) | data formatting | bytes 1703936 | tf_op jit(solution)/shard_map/reshape | solution.py:55
  25.4 4.9 %all-to-all-start = ((bf16[4,2,13,4096]{3,1,2,0:T(2,128)(2,1)}), bf16[4,2,13,4096]{3,1,2,0:T(2,128)(2,1)S(1)}, u32[]{:S(2)}, u32[]{:S(2)}) async-start(bf16[4,2,13,4096]{3,1,2,0:T(2,128)(2,1)} %copy.43), calls=%async_computation | async-start | bytes 1703936 | tf_op jit(solution)/shard_map/all_to_all | solution.py:56
  30.3 6.2 %copy.47 = bf16[2,128,4096]{1,0,2:T(2,128)(2,1)} copy(bf16[2,128,4096]{2,1,0:T(8,128)(2,1)} %param.16) | data formatting | bytes 4194304 | tf_op args[6]
  36.5 15.8 %all-to-all-done = bf16[4,2,13,4096]{3,1,2,0:T(2,128)(2,1)S(1)} async-done(((bf16[4,2,13,4096]{3,1,2,0:T(2,128)(2,1)}), bf16[4,2,13,4096]{3,1,2,0:T(2,128)(2,1)S(1)}, u32[]{:S(2)}, u32[]{:S(2)}) %all-to-all-start) | async-done | bytes 852000 | tf_op jit(solution)/shard_map/all_to_all | solution.py:56
  52.3 4.3 %all-to-all-start.1 = ((bf16[2,128,4096]{1,0,2:T(2,128)(2,1)}), bf16[2,128,4096]{1,0,2:T(2,128)(2,1)}, u32[]{:S(2)}, u32[]{:S(2)}) async-start(bf16[2,128,4096]{1,0,2:T(2,128)(2,1)} %copy.47), calls=%async_computation.1 | async-start | bytes 4194304 | tf_op jit(solution)/shard_map/all_to_all | solution.py:38
  56.7 0.0 reduce-scatter.2.cloned.1.call-start
  56.7 1.6 %fusion.43 = f32[16,128]{1,0:T(8,128)S(1)} fusion(bf16[128,4096]{1,0:T(8,128)(2,1)} %param.17, bf16[16,4096]{1,0:T(8,128)(2,1)S(1)} %all_gather.6, f32[4096]{0:T(1024)S(1)} %copy-done.2, f32[16]{0:T(128)S(1)} %add_rsqrt_fusion), kind=kOutput, calls=%fused_computation.43 | convolution fusion | flops 17039360 | bytes 1204288 | tf_op jit(solution)/shard_map/dot_general | solution.py:63
  58.4 3.1 %convolution_convert_fusion.1 = bf16[16,4096]{1,0:T(8,128)(2,1)} fusion(bf16[128,4096]{1,0:T(8,128)(2,1)} %param.19, bf16[128,4096]{1,0:T(8,128)(2,1)} %param.18, f32[16,128]{1,0:T(8,128)S(1)} %fusion.43, bf16[16,4096]{1,0:T(8,128)(2,1)S(1)} %all_gather.6, f32[4096]{0:T(1024)S(1)} %copy-done.2, f32[16]{0:T(128)S(1)} %add_rsqrt_fusion), kind=kOutput, calls=%fused_computation.1 | convolution fusion | flops 33894400 | bytes 2383936 | tf_op jit(solution)/shard_map/dot_general | solution.py:66
  61.6 0.8 fusion.12
  62.4 0.7 copy-done.1
  63.1 0.9 fusion.21
  64.0 22.9 %all_gather.7 = bf16[4,2,13,1024]{3,2,0,1:T(8,128)(2,1)S(1)} all-gather(bf16[4,2,13,128]{3,2,0,1:T(8,128)(2,1)S(1)} %fusion.21), channel_id=1, replica_groups=mesh['ep'=4,'tp'=8] {'tp'}, dimensions={3}, use_global_device_ids=true | all-gather | bytes 239616 | tf_op jit(solution)/shard_map/all_gather | solution.py:69
  86.9 0.2 reshape.39
  87.1 6.2 %copy.49 = bf16[2,128,8,512]{3,1,2,0:T(8,128)(2,1)} copy(bf16[2,128,8,512]{1,0,3,2:T(2,128)(2,1)} %bitcast.6) | data formatting | bytes 4194304 | tf_op jit(solution)/shard_map/all_to_all | solution.py:38
  93.2 2.1 %fusion.9 = bf16[2,4,13,512]{3,2,1,0:T(8,128)(2,1)S(1)} fusion(bf16[2,128,8,512]{3,1,2,0:T(8,128)(2,1)} %copy.49, bf16[4,2,13,8,128]{4,3,2,0,1:T(8,128)(2,1)S(1)} %reshape.39), kind=kOutput, calls=%fused_computation.9 | convolution fusion | flops 109850624 | bytes 2416640 | tf_op jit(solution)/shard_map/secpf,epfd->secpd/dot_general | solution.py:74
  95.3 0.8 copy.51
  96.1 3.3 %all-to-all-start.2 = ((bf16[4,2,13,512]{3,1,2,0:T(2,128)(2,1)}), bf16[4,2,13,512]{3,1,2,0:T(2,128)(2,1)S(1)}, u32[]{:S(2)}, u32[]{:S(2)}) async-start(bf16[4,2,13,512]{3,1,2,0:T(2,128)(2,1)} %copy.51), calls=%async_computation.2 | async-start | bytes 212992 | tf_op jit(solution)/shard_map/all_to_all | solution.py:81
  99.4 0.1 select_reduce_fusion
  99.5 6.0 %all-to-all-done.2 = bf16[4,2,13,512]{3,1,2,0:T(2,128)(2,1)S(1)} async-done(((bf16[4,2,13,512]{3,1,2,0:T(2,128)(2,1)}), bf16[4,2,13,512]{3,1,2,0:T(2,128)(2,1)S(1)}, u32[]{:S(2)}, u32[]{:S(2)}) %all-to-all-start.2) | async-done | bytes 106528 | tf_op jit(solution)/shard_map/all_to_all | solution.py:81
  105.5 0.1 reshape.35
  105.5 0.0 reduce-scatter.2.cloned.1.call-done
  105.6 1.5 %fusion.24 = bf16[16,512]{1,0:T(8,128)(2,1)} fusion(f32[16,104]{1,0:T(8,128)S(1)} %select_reduce_fusion, bf16[104,512]{1,0:T(8,128)(2,1)S(1)} %reshape.35, bf16[16,512]{1,0:T(8,128)(2,1)} %reduce-scatter.2.cloned.1.call-done), kind=kOutput, calls=%fused_computation.15 | convolution fusion | flops 10248192 | bytes 145920 | tf_op jit(solution)/shard_map/dot_general | solution.py:83
  (13 shorter events, 0.1 us)
Async XLA Ops:
  6.5 55.0 %copy-start = (bf16[2,128,4096]{2,1,0:T(8,128)(2,1)S(1)}, bf16[2,128,4096]{2,1,0:T(8,128)(2,1)}, u32[]{:S(2)}) copy-start(bf16[2,128,4096]{2,1,0:T(8,128)(2,1)} %param.14) | copy-start | bytes 6291460
  25.4 26.9 %all-to-all-start = ((bf16[4,2,13,4096]{3,1,2,0:T(2,128)(2,1)}), bf16[4,2,13,4096]{3,1,2,0:T(2,128)(2,1)S(1)}, u32[]{:S(2)}, u32[]{:S(2)}) async-start(bf16[4,2,13,4096]{3,1,2,0:T(2,128)(2,1)} %copy.43), calls=%async_computation | async-start | bytes 1703936 | tf_op jit(solution)/shard_map/all_to_all | solution.py:56
  36.5 20.2 %copy-start.2 = (f32[4096]{0:T(1024)S(1)}, f32[4096]{0:T(1024)}, u32[]{:S(2)}) copy-start(f32[4096]{0:T(1024)} %param.11) | copy-start | bytes 49156
  52.3 34.8 %all-to-all-start.1 = ((bf16[2,128,4096]{1,0,2:T(2,128)(2,1)}), bf16[2,128,4096]{1,0,2:T(2,128)(2,1)}, u32[]{:S(2)}, u32[]{:S(2)}) async-start(bf16[2,128,4096]{1,0,2:T(2,128)(2,1)} %copy.47), calls=%async_computation.1 | async-start | bytes 4194304 | tf_op jit(solution)/shard_map/all_to_all | solution.py:38
  56.7 48.9 %reduce-scatter.2.cloned.1.call-start = ((), (), s32[]{:S(2)}) async-start(), calls=%async_computation.4 | async-start | bytes 147456 | tf_op jit(solution)/shard_map/reduce_scatter | solution.py:78
  61.6 1.6 %copy-start.1 = (bf16[2,128,4096]{2,1,0:T(8,128)(2,1)S(1)}, bf16[2,128,4096]{2,1,0:T(8,128)(2,1)}, u32[]{:S(2)}) copy-start(bf16[2,128,4096]{2,1,0:T(8,128)(2,1)} %param.15) | copy-start | bytes 6291460
  93.2 6.1 %copy-start.3 = (f32[16,4]{0,1:T(4,128)S(1)}, f32[16,4]{0,1:T(4,128)}, u32[]{:S(2)}) copy-start(f32[16,4]{0,1:T(4,128)} %param.13) | copy-start | bytes 772
  96.1 9.4 %all-to-all-start.2 = ((bf16[4,2,13,512]{3,1,2,0:T(2,128)(2,1)}), bf16[4,2,13,512]{3,1,2,0:T(2,128)(2,1)S(1)}, u32[]{:S(2)}, u32[]{:S(2)}) async-start(bf16[4,2,13,512]{3,1,2,0:T(2,128)(2,1)} %copy.51), calls=%async_computation.2 | async-start | bytes 212992 | tf_op jit(solution)/shard_map/all_to_all | solution.py:81
Sparse Core Ops, SparseCore 0:
  61.7 33.0 reduce-scatter.1
where the time goes:
time: 115 us; the launch traced here: 114 us
  blocking collectives  33.8 us (29%)
  waiting for transfers between devices  21.8 us (19%)
  local copies, waits for them, and re-layouts  17.5 us (15%)
  between operations  13.5 us (12%)
  starting transfers between devices  12.6 us (11%)
  matrix products  12.1 us (11%)
  other arithmetic  2.59 us (2%)
    all_gather x1, blocking collectives, per_device(): inner_whole = lax.all_gather(inner_vals, 'tp', axis=3, tiled=True)  22.9 us
    all_to_all x1, waiting for transfers between devices, per_device(): lax.all_to_all(packed, 'ep', split_axis=0, concat_axis=0, tiled=True)  15.8 us
    all_gather x1, blocking collectives, per_device(): gathered = lax.all_gather(hidden, 'tp', axis=1, tiled=True)  10.9 us
    unnamed x9, local copies, waits for them, and re-layouts  6.96 us
    all_to_all x1, local copies, waits for them, and re-layouts, per_device(): lax.all_to_all(down_weight, 'tp', split_axis=2, concat_axis=1, tiled=True)  6.15 us
    all_to_all x1, waiting for transfers between devices, per_device(): lax.all_to_all(answers, 'ep', split_axis=0, concat_axis=0, tiled=True)  5.96 us
    all_to_all x1, starting transfers between devices, per_device(): lax.all_to_all(packed, 'ep', split_axis=0, concat_axis=0, tiled=True)  4.87 us
    all_to_all x1, starting transfers between devices, per_device(): lax.all_to_all(down_weight, 'tp', split_axis=2, concat_axis=1, tiled=True)  4.34 us
  transfers between devices with their start and end apart: 4, of which 2 were waited for; matrix products, arithmetic and copies ran while one was open for 19% of the time, Pallas kernels for 0%

commit v1 on v0

v1 whole, which is shorter than its diff:
```python
import functools

import jax
import jax.numpy as jnp
from jax import lax
from jax.experimental import pallas as pl
from jax.experimental.pallas import tpu as pltpu
from jax.sharding import PartitionSpec as P

MESH = pl.DeviceIdType.MESH
norm_eps = 1e-06
NT = (((1,), (1,)), ((), ()))
F32 = jnp.float32
BF16 = jnp.bfloat16


def flip(index, bits, count):
    if count & (count - 1):
        return lax.rem(index + bits, count)
    result, place = 0, 1
    while place < count:
        digit = lax.rem(index // place, 2)
        if (bits // place) % 2:
            digit = 1 - digit
        result = result + digit * place
        place *= 2
    return result


def unflip(index, bits, count):
    if count & (count - 1):
        return lax.rem(index + count - bits, count)
    return flip(index, bits, count)


def far_first(count):
    return sorted(range(count), key=lambda step: -min(step, count - step))


def kernel(
    groups,
    width,
    cores,
    shared_split,
    hidden_hbm,
    gain_hbm,
    routes_hbm,
    rw_hbm,
    gate_hbm,
    up_hbm,
    down_hbm,
    sgate_hbm,
    sup_hbm,
    sdown_hbm,
    out_ref,
    xbuf,
    gain,
    routes,
    rw,
    table,
    gate_w,
    up_w,
    down_w,
    sgate_w,
    sup_w,
    sdown_w,
    acc_g,
    acc_u,
    acc_sg,
    acc_su,
    acc_ss,
    core_send,
    core_recv,
    plane_send,
    plane_recv,
    total,
    z_send,
    z_recv,
    load_sem,
    zs_sem,
    zr_sem,
    ts_sem,
    tr_sem,
    ps_sem,
    pr_sem,
    ds_sem,
    dr_sem,
    cs_sem,
    cr_sem,
    qs_sem,
    qr_sem,
    ys_sem,
    yr_sem,
):
    e = lax.axis_index("ep")
    p = lax.axis_index("tp")
    chips = width // cores
    q, c = p // cores, lax.rem(p, cores)
    rows, feats = hidden_hbm.shape
    tokens = rows * groups
    local, units, _ = gate_hbm.shape
    split_units = sgate_w.shape[0]

    def at_chip(chip, core):
        return chip * cores + core

    def block(index):
        return pl.ds(pl.multiple_of(index * rows, rows), rows)

    def columns(index):
        return pl.ds(pl.multiple_of(index * feats, feats), feats)

    loads = [
        pltpu.make_async_copy(hidden_hbm, xbuf.at[p, block(e)], load_sem.at[0]),
        pltpu.make_async_copy(routes_hbm, routes, load_sem.at[1]),
        pltpu.make_async_copy(rw_hbm, rw, load_sem.at[2]),
        pltpu.make_async_copy(gain_hbm, gain, load_sem.at[3]),
    ]
    part = pl.ds(
        pl.multiple_of(e * split_units, split_units) if shared_split else 0, split_units
    )
    number = len(loads)
    for index in range(local):
        span = pl.ds(index * units, units)
        for source, target in ((gate_hbm, gate_w), (up_hbm, up_w)):
            loads.append(
                pltpu.make_async_copy(source.at[index], target.at[span], load_sem.at[len(loads)])
            )
    for source, target in ((sgate_hbm, sgate_w), (sup_hbm, sup_w)):
        loads.append(pltpu.make_async_copy(source.at[part], target, load_sem.at[len(loads)]))
    first_done = len(loads)
    for index in range(local):
        span = pl.ds(index * units, units)
        loads.append(
            pltpu.make_async_copy(down_hbm.at[index], down_w.at[span], load_sem.at[len(loads)])
        )
    loads.append(pltpu.make_async_copy(sdown_hbm.at[part], sdown_w, load_sem.at[len(loads)]))
    for load in loads:
        load.start()

    barrier = pltpu.get_barrier_semaphore()
    partners = [(lax.rem(e + step, groups), p) for step in range(1, groups)]
    partners += [(e, at_chip(flip(q, d, chips), c)) for d in range(1, chips)]
    partners += [(e, at_chip(q, lax.rem(c + step, cores))) for step in range(1, cores)]
    for partner in partners:
        pl.semaphore_signal(barrier, inc=1, device_id=partner, device_id_type=MESH)

    loads[1].wait()
    loads[2].wait()
    lane = lax.broadcasted_iota(jnp.int32, (rows, table.shape[2]), 1)
    dense = jnp.zeros((rows, table.shape[2]), F32)
    for k in range(routes.shape[1]):
        dense = dense + jnp.where(lane == routes[:, k : k + 1], rw[:, k : k + 1], 0.0)
    table[e] = dense
    loads[0].wait()
    pl.semaphore_wait(barrier, len(partners))

    sends = []

    def remote(source, target, send, recv, device, go=True):
        copy = pltpu.make_async_remote_copy(
            src_ref=source,
            dst_ref=target,
            send_sem=send,
            recv_sem=recv,
            device_id=device,
            device_id_type=MESH,
        )
        if go:
            copy.start()
            sends.append(copy)
        return copy

    for step in far_first(groups):
        if step:
            mine = xbuf.at[p, block(e)]
            remote(mine, mine, zs_sem.at[step], zr_sem.at[step], (lax.rem(e + step, groups), p))
    if groups * chips <= 32:
        pieces = [[step] for step in [0] + far_first(groups)[::-1] if step or True]
        pieces = [[0]] + [[step] for step in far_first(groups)[::-1] if step]
    else:
        pieces = [list(range(groups))]

    def piece_rows(piece):
        if len(piece) > 1:
            return pl.ds(0, tokens)
        return block(lax.rem(e + groups - piece[0], groups))

    core_next = lax.rem(c + 1, cores)
    for number, piece in enumerate(pieces):
        for step in piece:
            if step:
                theirs = xbuf.at[p, block(lax.rem(e + groups - step, groups))]
                remote(theirs, theirs, zs_sem.at[step], zr_sem.at[step], (e, p), False).wait_recv()
        view = xbuf.at[p, piece_rows(piece)]
        for d in range(chips - 1, 0, -1):
            remote(
                view,
                view,
                ps_sem.at[number, d],
                pr_sem.at[number, d],
                (e, at_chip(flip(q, d, chips), c)),
            )
        remote(view, view, ds_sem.at[number, 0], dr_sem.at[number, 0], (e, at_chip(q, core_next)))
        if number == 0:
            for step in far_first(groups):
                if step:
                    remote(
                        table.at[e],
                        table.at[e],
                        ts_sem.at[step],
                        tr_sem.at[step],
                        (lax.rem(e + step, groups), p),
                    )

    def project(owner, first):
        values = xbuf[owner].astype(F32)
        scaled = (values * gain[:, columns(owner)]).astype(BF16)
        squares = values * values
        partial = squares[:, :128]
        for start in range(128, feats, 128):
            partial = partial + squares[:, start : start + 128]
        for acc, weight in (
            (acc_g, gate_w),
            (acc_u, up_w),
            (acc_sg, sgate_w),
            (acc_su, sup_w),
        ):
            product = lax.dot_general(
                scaled, weight[:, columns(owner)], NT, preferred_element_type=F32
            )
            acc[...] = product if first else acc[...] + product
        acc_ss[...] = partial if first else acc_ss[...] + partial

    for load in loads[3:first_done]:
        load.wait()
    project(p, True)

    for d in range(1, chips):
        owner = at_chip(unflip(q, d, chips), c)
        for number, piece in enumerate(pieces):
            view = xbuf.at[owner, piece_rows(piece)]
            remote(view, view, ps_sem.at[number, d], pr_sem.at[number, d], (e, p), False).wait_recv()
            remote(
                view, view, ds_sem.at[number, d], dr_sem.at[number, d], (e, at_chip(q, core_next))
            )
        project(owner, False)
    for d in range(chips):
        owner = at_chip(unflip(q, d, chips), core_next)
        for number, piece in enumerate(pieces):
            view = xbuf.at[owner, piece_rows(piece)]
            remote(view, view, ds_sem.at[number, d], dr_sem.at[number, d], (e, p), False).wait_recv()
        project(owner, False)

    for step in range(1, groups):
        theirs = table.at[lax.rem(e + groups - step, groups)]
        remote(theirs, theirs, ts_sem.at[step], tr_sem.at[step], (e, p), False).wait_recv()

    inv = lax.rsqrt(jnp.sum(acc_ss[...], axis=1, keepdims=True) / (feats * width) + norm_eps)
    tables = table[...].reshape(tokens, table.shape[2])
    lanes = lax.broadcasted_iota(jnp.int32, tables.shape, 1)
    unit = lax.broadcasted_iota(jnp.int32, (tokens, local * units), 1)
    mix = jnp.zeros((tokens, local * units), F32)
    for index in range(local):
        mine = jnp.sum(
            jnp.where(lanes == e * local + index, tables, 0.0), axis=1, keepdims=True
        )
        inside = (unit >= index * units) & (unit < (index + 1) * units)
        mix = jnp.where(inside, mine, mix)

    def swish(v):
        return v / (1.0 + jnp.exp(-v))

    inner = (swish(acc_g[...] * inv) * (acc_u[...] * inv) * mix).astype(BF16)
    shared = swish(acc_sg[...] * inv) * (acc_su[...] * inv)
    if not shared_split:
        row = lax.broadcasted_iota(jnp.int32, shared.shape, 0)
        shared = jnp.where((row >= e * rows) & (row < (e + 1) * rows), shared, 0.0)
    shared = shared.astype(BF16)
    for load in loads[first_done:]:
        load.wait()

    def expand(owner):
        return jnp.dot(
            inner, down_w[:, columns(owner)], preferred_element_type=F32
        ) + jnp.dot(shared, sdown_w[:, columns(owner)], preferred_element_type=F32)

    order = list(range(chips - 1, -1, -1))
    for d in order:
        core_send[d] = expand(at_chip(flip(q, d, chips), core_next)).astype(BF16)
        remote(
            core_send.at[d], core_recv.at[d], cs_sem.at[d], cr_sem.at[d], (e, at_chip(q, core_next))
        )
    if len(pieces) > 1:
        out_pieces = [[step] for step in far_first(groups)]
    else:
        out_pieces = pieces

    def out_rows(piece):
        if len(piece) > 1:
            return pl.ds(0, tokens)
        return block(lax.rem(e + piece[0], groups))

    for d in order:
        value = expand(at_chip(flip(q, d, chips), c))
        remote(
            core_send.at[d], core_recv.at[d], cs_sem.at[d], cr_sem.at[d], (e, p), False
        ).wait_recv()
        value = value + core_recv[d].astype(F32)
        if d == 0:
            total[...] = value
        else:
            plane_send[d] = value.astype(BF16)
            for number, piece in enumerate(out_pieces):
                remote(
                    plane_send.at[d, out_rows(piece)],
                    plane_recv.at[d, out_rows(piece)],
                    qs_sem.at[number, d],
                    qr_sem.at[number, d],
                    (e, at_chip(flip(q, d, chips), c)),
                )
    for number, piece in enumerate(out_pieces):
        for d in range(1, chips):
            view = plane_recv.at[d, out_rows(piece)]
            remote(view, view, qs_sem.at[number, d], qr_sem.at[number, d], (e, p), False).wait_recv()
        for step in piece:
            span = block(lax.rem(e + step, groups))
            value = total[span, :]
            for d in range(1, chips):
                value = value + plane_recv[d, span, :].astype(F32)
            if step:
                z_send[step] = value.astype(BF16)
                remote(
                    z_send.at[step],
                    z_recv.at[step],
                    ys_sem.at[step],
                    yr_sem.at[step],
                    (lax.rem(e + step, groups), p),
                )
            else:
                total[span, :] = value
    answer = total[block(e), :]
    for step in range(1, groups):
        remote(
            z_send.at[step], z_recv.at[step], ys_sem.at[step], yr_sem.at[step], (e, p), False
        ).wait_recv()
        answer = answer + z_recv[step].astype(F32)
    out_ref[...] = answer.astype(BF16)
    for copy in sends:
        copy.wait_send()


def solution(mesh):
    groups, width = mesh.shape["ep"], mesh.shape["tp"]
    cores = 2

    def step(hidden, gain, routes, rw, gate, up, down, sgate, sup, sdown):
        rows, feats = hidden.shape
        local, units, model = gate.shape
        tokens = rows * groups
        chips = width // cores
        shared_units = sgate.shape[0]
        shared_split = shared_units % (16 * groups) == 0
        split_units = shared_units // groups if shared_split else shared_units
        lanes = -(-local * groups // 128) * 128
        count = groups if groups * chips <= 32 else 1
        dma = pltpu.SemaphoreType.DMA
        any_spec = pl.BlockSpec(memory_space=pl.ANY)
        return pl.pallas_call(
            functools.partial(kernel, groups, width, cores, shared_split),
            out_shape=jax.ShapeDtypeStruct((rows, feats), BF16),
            in_specs=[any_spec] * 10,
            out_specs=pl.BlockSpec(memory_space=pltpu.VMEM),
            scratch_shapes=[
                pltpu.VMEM((width, tokens, feats), BF16),
                pltpu.VMEM((1, model), F32),
                pltpu.VMEM(routes.shape, jnp.int32),
                pltpu.VMEM(rw.shape, F32),
                pltpu.VMEM((groups, rows, lanes), F32),
                pltpu.VMEM((local * units, model), BF16),
                pltpu.VMEM((local * units, model), BF16),
                pltpu.VMEM((local * units, model), BF16),
                pltpu.VMEM((split_units, model), BF16),
                pltpu.VMEM((split_units, model), BF16),
                pltpu.VMEM((split_units, model), BF16),
                pltpu.VMEM((tokens, local * units), F32),
                pltpu.VMEM((tokens, local * units), F32),
                pltpu.VMEM((tokens, split_units), F32),
                pltpu.VMEM((tokens, split_units), F32),
                pltpu.VMEM((tokens, 128), F32),
                pltpu.VMEM((chips, tokens, feats), BF16),
                pltpu.VMEM((chips, tokens, feats), BF16),
                pltpu.VMEM((chips, tokens, feats), BF16),
                pltpu.VMEM((chips, tokens, feats), BF16),
                pltpu.VMEM((tokens, feats), F32),
                pltpu.VMEM((groups, rows, feats), BF16),
                pltpu.VMEM((groups, rows, feats), BF16),
                dma((4 + 3 * local + 3,)),
                dma((groups,)),
                dma((groups,)),
                dma((groups,)),
                dma((groups,)),
                dma((count, chips)),
                dma((count, chips)),
                dma((count, chips)),
                dma((count, chips)),
                dma((chips,)),
                dma((chips,)),
                dma((count, chips)),
                dma((count, chips)),
                dma((groups,)),
                dma((groups,)),
            ],
            compiler_params=pltpu.CompilerParams(
                collective_id=0,
                has_side_effects=True,
                vmem_limit_bytes=60 * 1024 * 1024,
            ),
            name="moe_step",
        )(hidden, gain.reshape(1, -1), routes, rw, gate, up, down, sgate, sup, sdown)

    in_specs = (
        P("ep", "tp"),
        P(),
        P("ep", None),
        P("ep", None),
        P("ep", "tp", None),
        P("ep", "tp", None),
        P("ep", "tp", None),
        P("tp", None),
        P("tp", None),
        P("tp", None),
    )
    return jax.shard_map(
        step, mesh=mesh, in_specs=in_specs, out_specs=P("ep", "tp"), check_vma=False
    )
```

time: 115 us -> 31.4 us (0.27)
  blocking collectives: 33.8 us -> 0 us
  Pallas kernels: 0 us -> 27.1 us
  waiting for transfers between devices: 21.8 us -> 0 us
  between operations: 13.5 us -> 0.01 us
  local copies, waits for them, and re-layouts: 17.5 us -> 4.02 us
  starting transfers between devices: 12.6 us -> 0 us
  matrix products: 12.1 us -> 0 us
  other arithmetic: 2.59 us -> 0 us
    all_gather x2 -> x0, blocking collectives: 33.8 us -> none  [the longest x1 22.9 us: per_device(): inner_whole = lax.all_gather(inner_vals, 'tp', axis=3, tiled=True)]
    pallas_call x0 -> x1, Pallas kernels: none -> 27.1 us  [step(): pl.pallas_call(functools.partial(kernel, groups, width, cores, shared_spl...]
    all_to_all x3 -> x0, waiting for transfers between devices: 21.8 us -> none  [the longest x1 15.8 us: per_device(): lax.all_to_all(packed, 'ep', split_axis=0, concat_axis=0, tiled=True)]
    all_to_all x3 -> x0, starting transfers between devices: 12.5 us -> none  [the longest x1 4.87 us: per_device(): lax.all_to_all(packed, 'ep', split_axis=0, concat_axis=0, tiled=True)]
    dot_general x7 -> x0, matrix products: 12.1 us -> none  [the longest x1 3.14 us: per_device(): jnp.dot(shared_inner, shared_down, preferred_element_type=jnp.float32)]
    all_to_all x2 -> x0, local copies, waits for them, and re-layouts: 6.17 us -> none  [the longest x1 6.15 us: per_device(): lax.all_to_all(down_weight, 'tp', split_axis=2, concat_axis=1, tiled=True)]
    reshape x4 -> x0, local copies, waits for them, and re-layouts: 3.5 us -> none  [the longest x2 3.28 us: per_device(): packed = packed.reshape(groups, local_experts, capacity, full_width)]
    unnamed x9 -> x3, local copies, waits for them, and re-layouts: 6.96 us -> 4.02 us
  transfers between devices with their start and end apart: 4 -> 0, of which waited for: 2 -> 0; matrix products, arithmetic and copies ran while one was open for 19% -> 0% of each run, Pallas kernels for 0% -> 0%
where the time goes in v1:
time: 31.4 us; the launch traced here: 31.1 us
  Pallas kernels  27.1 us (86%)
  local copies, waits for them, and re-layouts  4.02 us (13%)
    pallas_call x1, Pallas kernels, step(): pl.pallas_call(functools.partial(kernel, groups, width, cores, shared_spl...  27.1 us
    unnamed x3, local copies, waits for them, and re-layouts  4.02 us

profile of v1, /device:TPU:0, one launch (start us, length us, event | category | flops | bytes accessed | tf_op | source)
XLA Modules:
  0.0 31.1 jit_solution(775306644942850129)
XLA Ops:
  0.0 1.4 %copy.11.routes_hbm = s32[16,4]{1,0:T(8,128)} copy(s32[16,4]{0,1:T(4,128)} %param.12) | data formatting | bytes 512 | tf_op args[2]
  1.4 1.3 %copy.12.rw_hbm = f32[16,4]{1,0:T(8,128)} copy(f32[16,4]{0,1:T(4,128)} %param.13) | data formatting | bytes 512 | tf_op args[3]
  2.7 27.1 %moe_step.1 = bf16[16,512]{1,0:T(8,128)(2,1)} custom-call(bf16[16,512]{1,0:T(8,128)(2,1)} %hidden_hbm.1, f32[1,4096]{1,0:T(1,128)} %bitcast.1, s32[16,4]{1,0:T(8,128)} %copy.11.routes_hbm, f32[16,4]{1,0:T(8,128)} %copy.12.rw_hbm, bf16[2,128,4096]{2,1,0:T(8,128)(2,1)} %gate_hbm.1, bf16[2,128,4096]{2,1,0:T(8,128)(2,1)} %up_hbm.1, ...), custom_call_target="tpu_custom_call" | custom-call | tf_op jit(solution)/shard_map/moe_step/pallas_call | solution.py:369
  29.8 1.3 %copy.14 = bf16[16,512]{1,0:T(8,128)(2,1)} copy(bf16[16,512]{1,0:T(8,128)(2,1)} %moe_step.1) | data formatting | bytes 32768

commit v2 on v1

--- a/solution.py
+++ b/solution.py
@@ -149,8 +149,9 @@
     loads[2].wait()
     lane = lax.broadcasted_iota(jnp.int32, (rows, table.shape[2]), 1)
     dense = jnp.zeros((rows, table.shape[2]), F32)
-    for k in range(routes.shape[1]):
-        dense = dense + jnp.where(lane == routes[:, k : k + 1], rw[:, k : k + 1], 0.0)
+    chosen, strength = jnp.transpose(routes[...]), jnp.transpose(rw[...])
+    for k in range(routes.shape[0]):
+        dense = dense + jnp.where(lane == chosen[:, k : k + 1], strength[:, k : k + 1], 0.0)
     table[e] = dense
     loads[0].wait()
     pl.semaphore_wait(barrier, len(partners))
@@ -176,7 +177,6 @@
             mine = xbuf.at[p, block(e)]
             remote(mine, mine, zs_sem.at[step], zr_sem.at[step], (lax.rem(e + step, groups), p))
     if groups * chips <= 32:
-        pieces = [[step] for step in [0] + far_first(groups)[::-1] if step or True]
         pieces = [[0]] + [[step] for step in far_first(groups)[::-1] if step]
     else:
         pieces = [list(range(groups))]
@@ -374,8 +374,8 @@
             scratch_shapes=[
                 pltpu.VMEM((width, tokens, feats), BF16),
                 pltpu.VMEM((1, model), F32),
-                pltpu.VMEM(routes.shape, jnp.int32),
-                pltpu.VMEM(rw.shape, F32),
+                pltpu.VMEM(routes.shape[::-1], jnp.int32),
+                pltpu.VMEM(rw.shape[::-1], F32),
                 pltpu.VMEM((groups, rows, lanes), F32),
                 pltpu.VMEM((local * units, model), BF16),
                 pltpu.VMEM((local * units, model), BF16),
@@ -417,7 +417,7 @@
                 vmem_limit_bytes=60 * 1024 * 1024,
             ),
             name="moe_step",
-        )(hidden, gain.reshape(1, -1), routes, rw, gate, up, down, sgate, sup, sdown)
+        )(hidden, gain.reshape(1, -1), routes.T, rw.T, gate, up, down, sgate, sup, sdown)
 
     in_specs = (
         P("ep", "tp"),

time: 31.4 us -> 28.7 us (0.914)
  local copies, waits for them, and re-layouts: 4.02 us -> 1.32 us
    unnamed x3 -> x1, local copies, waits for them, and re-layouts: 4.02 us -> 1.32 us
where the time goes in v2:
time: 28.7 us; the launch traced here: 28.4 us
  Pallas kernels  27.1 us (94%)
  local copies, waits for them, and re-layouts  1.32 us (5%)
    pallas_call x1, Pallas kernels, step(): pl.pallas_call(functools.partial(kernel, groups, width, cores, shared_spl...  27.1 us
    unnamed x1, local copies, waits for them, and re-layouts  1.32 us

profile of v2, /device:TPU:0, one launch (start us, length us, event | category | flops | bytes accessed | tf_op | source)
XLA Modules:
  0.0 28.4 jit_solution(181896486742359751)
XLA Ops:
  0.0 27.1 %moe_step.1 = bf16[16,512]{1,0:T(8,128)(2,1)} custom-call(bf16[16,512]{1,0:T(8,128)(2,1)} %hidden_hbm.1, f32[1,4096]{1,0:T(1,128)} %bitcast.3, s32[4,16]{1,0:T(4,128)} %bitcast.4, f32[4,16]{1,0:T(4,128)} %bitcast.5, bf16[2,128,4096]{2,1,0:T(8,128)(2,1)} %gate_hbm.1, bf16[2,128,4096]{2,1,0:T(8,128)(2,1)} %up_hbm.1, bf16[2,128,4096]{2,1,0:T(8,128)(2,1)} %down_hbm.1, ...), custom_call_target="tpu_custom_call" | custom-call | tf_op jit(solution)/shard_map/moe_step/pallas_call | solution.py:369
  27.1 1.3 %copy.12 = bf16[16,512]{1,0:T(8,128)(2,1)} copy(bf16[16,512]{1,0:T(8,128)(2,1)} %moe_step.1) | data formatting | bytes 32768

commit v3 on v2

--- a/solution.py
+++ b/solution.py
@@ -236,6 +236,13 @@
         load.wait()
     project(p, True)
 
+    def forwarded(d):
+        owner = at_chip(unflip(q, d, chips), core_next)
+        for number, piece in enumerate(pieces):
+            view = xbuf.at[owner, piece_rows(piece)]
+            remote(view, view, ds_sem.at[number, d], dr_sem.at[number, d], (e, p), False).wait_recv()
+        project(owner, False)
+
     for d in range(1, chips):
         owner = at_chip(unflip(q, d, chips), c)
         for number, piece in enumerate(pieces):
@@ -245,12 +252,10 @@
                 view, view, ds_sem.at[number, d], dr_sem.at[number, d], (e, at_chip(q, core_next))
             )
         project(owner, False)
-    for d in range(chips):
-        owner = at_chip(unflip(q, d, chips), core_next)
-        for number, piece in enumerate(pieces):
-            view = xbuf.at[owner, piece_rows(piece)]
-            remote(view, view, ds_sem.at[number, d], dr_sem.at[number, d], (e, p), False).wait_recv()
-        project(owner, False)
+        if d > 1:
+            forwarded(d - 2)
+    for d in range(max(chips - 2, 0), chips):
+        forwarded(d)
 
     for step in range(1, groups):
         theirs = table.at[lax.rem(e + groups - step, groups)]
@@ -311,14 +316,16 @@
             total[...] = value
         else:
             plane_send[d] = value.astype(BF16)
+        if d == 1:
             for number, piece in enumerate(out_pieces):
-                remote(
-                    plane_send.at[d, out_rows(piece)],
-                    plane_recv.at[d, out_rows(piece)],
-                    qs_sem.at[number, d],
-                    qr_sem.at[number, d],
-                    (e, at_chip(flip(q, d, chips), c)),
-                )
+                for peer in order[:-1]:
+                    remote(
+                        plane_send.at[peer, out_rows(piece)],
+                        plane_recv.at[peer, out_rows(piece)],
+                        qs_sem.at[number, peer],
+                        qr_sem.at[number, peer],
+                        (e, at_chip(flip(q, peer, chips), c)),
+                    )
     for number, piece in enumerate(out_pieces):
         for d in range(1, chips):
             view = plane_recv.at[d, out_rows(piece)]
@@ -368,7 +375,7 @@
         any_spec = pl.BlockSpec(memory_space=pl.ANY)
         return pl.pallas_call(
             functools.partial(kernel, groups, width, cores, shared_split),
-            out_shape=jax.ShapeDtypeStruct((rows, feats), BF16),
+            out_shape=pltpu.VMEM((rows, feats), BF16),
             in_specs=[any_spec] * 10,
             out_specs=pl.BlockSpec(memory_space=pltpu.VMEM),
             scratch_shapes=[

time: 28.7 us -> 27.4 us (0.955)
  local copies, waits for them, and re-layouts: 1.32 us -> 0.61 us
  Pallas kernels: 27.1 us -> 26.6 us
    unnamed x1, local copies, waits for them, and re-layouts: 1.32 us -> 0.61 us
    pallas_call x1, Pallas kernels: 27.1 us -> 26.6 us  [step(): pl.pallas_call(functools.partial(kernel, groups, width, cores, shared_spl...]
where the time goes in v3:
time: 27.4 us; the launch traced here: 27.2 us
  Pallas kernels  26.6 us (97%)
  local copies, waits for them, and re-layouts  0.61 us (2%)
    pallas_call x1, Pallas kernels, step(): pl.pallas_call(functools.partial(kernel, groups, width, cores, shared_spl...  26.6 us
    unnamed x1, local copies, waits for them, and re-layouts  0.61 us

profile of v3, /device:TPU:0, one launch (start us, length us, event | category | flops | bytes accessed | tf_op | source)
XLA Modules:
  0.0 27.2 jit_solution(11900476689248731477)
XLA Ops:
  0.0 26.6 %moe_step.1 = bf16[16,512]{1,0:T(8,128)(2,1)S(1)} custom-call(bf16[16,512]{1,0:T(8,128)(2,1)} %hidden_hbm.1, f32[1,4096]{1,0:T(1,128)} %bitcast.3, s32[4,16]{1,0:T(4,128)} %bitcast.4, f32[4,16]{1,0:T(4,128)} %bitcast.5, bf16[2,128,4096]{2,1,0:T(8,128)(2,1)} %gate_hbm.1, bf16[2,128,4096]{2,1,0:T(8,128)(2,1)} %up_hbm.1, bf16[2,128,4096]{2,1,0:T(8,128)(2,1)} %down_hbm.1, ...), custom_call_target="tpu_custom_call" | custom-call | tf_op jit(solution)/shard_map/moe_step/pallas_call | solution.py:376
  26.6 0.6 %copy.12 = bf16[16,512]{1,0:T(8,128)(2,1)} copy(bf16[16,512]{1,0:T(8,128)(2,1)S(1)} %moe_step.1) | data formatting | bytes 32768

commit v4 on v3

--- a/solution.py
+++ b/solution.py
@@ -172,12 +172,22 @@
             sends.append(copy)
         return copy
 
-    for step in far_first(groups):
-        if step:
+    near, far = far_first(groups)[::-1], far_first(groups)
+    near, far = [step for step in near if step], [step for step in far if step]
+    if groups == 4:
+        low, high = (groups - 1 - e) // (groups - 1), e // (groups - 1)
+        near = [1 + 2 * low, 3 - low - high, 2 - low + high]
+        far = [2 + low - high, 3 - low - high, 1 + 2 * high]
+
+    def own(step):
+        return isinstance(step, int) and step == 0
+
+    for step in far:
+        if not own(step):
             mine = xbuf.at[p, block(e)]
             remote(mine, mine, zs_sem.at[step], zr_sem.at[step], (lax.rem(e + step, groups), p))
     if groups * chips <= 32:
-        pieces = [[0]] + [[step] for step in far_first(groups)[::-1] if step]
+        pieces = [[0]] + [[step] for step in near]
     else:
         pieces = [list(range(groups))]
 
@@ -189,7 +199,7 @@
     core_next = lax.rem(c + 1, cores)
     for number, piece in enumerate(pieces):
         for step in piece:
-            if step:
+            if not own(step):
                 theirs = xbuf.at[p, block(lax.rem(e + groups - step, groups))]
                 remote(theirs, theirs, zs_sem.at[step], zr_sem.at[step], (e, p), False).wait_recv()
         view = xbuf.at[p, piece_rows(piece)]
@@ -297,7 +307,7 @@
             core_send.at[d], core_recv.at[d], cs_sem.at[d], cr_sem.at[d], (e, at_chip(q, core_next))
         )
     if len(pieces) > 1:
-        out_pieces = [[step] for step in far_first(groups)]
+        out_pieces = [[step] for step in far] + [[0]]
     else:
         out_pieces = pieces
 
@@ -335,7 +345,7 @@
             value = total[span, :]
             for d in range(1, chips):
                 value = value + plane_recv[d, span, :].astype(F32)
-            if step:
+            if not own(step):
                 z_send[step] = value.astype(BF16)
                 remote(
                     z_send.at[step],

time: 27.4 us -> 25.7 us (0.938)
  Pallas kernels: 26.6 us -> 25 us
    pallas_call x1, Pallas kernels: 26.6 us -> 25 us  [step(): pl.pallas_call(functools.partial(kernel, groups, width, cores, shared_spl...]
where the time goes in v4:
time: 25.7 us; the launch traced here: 25.6 us
  Pallas kernels  25 us (97%)
  local copies, waits for them, and re-layouts  0.61 us (2%)
    pallas_call x1, Pallas kernels, step(): pl.pallas_call(functools.partial(kernel, groups, width, cores, shared_spl...  25 us
    unnamed x1, local copies, waits for them, and re-layouts  0.61 us

profile of v4, /device:TPU:0, one launch (start us, length us, event | category | flops | bytes accessed | tf_op | source)
XLA Modules:
  0.0 25.6 jit_solution(10545709705470385947)
XLA Ops:
  0.0 25.0 %moe_step.1 = bf16[16,512]{1,0:T(8,128)(2,1)S(1)} custom-call(bf16[16,512]{1,0:T(8,128)(2,1)} %hidden_hbm.1, f32[1,4096]{1,0:T(1,128)} %bitcast.3, s32[4,16]{1,0:T(4,128)} %bitcast.4, f32[4,16]{1,0:T(4,128)} %bitcast.5, bf16[2,128,4096]{2,1,0:T(8,128)(2,1)} %gate_hbm.1, bf16[2,128,4096]{2,1,0:T(8,128)(2,1)} %up_hbm.1, bf16[2,128,4096]{2,1,0:T(8,128)(2,1)} %down_hbm.1, ...), custom_call_target="tpu_custom_call" | custom-call | tf_op jit(solution)/shard_map/moe_step/pallas_call | solution.py:386
  25.0 0.6 %copy.12 = bf16[16,512]{1,0:T(8,128)(2,1)} copy(bf16[16,512]{1,0:T(8,128)(2,1)S(1)} %moe_step.1) | data formatting | bytes 32768
